TPU v7x, 32 devices: a whole 2x2x4 slice. The times are simulated.
32 devices in a mesh: ep: 4 (over y, x), tp: 8 (over z, core).
Axes of the slice: x: 2, y: 2, z: 4, core: 2. Of those that a mesh axis runs over, the one named last changes fastest.
Arguments:
- queries: bfloat16 [2048, 1024], P('ep', 'tp'), may hold values from -30 to 30
- key_vectors: bfloat16 [2048, 1024], P('ep', 'tp'), may hold values from -30 to 30
- value_vectors: bfloat16 [2048, 1024], P('ep', 'tp'), may hold values from -9 to 9
- cumulative_gate: float32 [2048, 16], P('ep', 'tp'), as said below
- out_weight: bfloat16 [1024, 2048], P('tp'), may hold values from -0.1875 to 0.1875
- expert_tokens: bfloat16 [3072, 2048], P(('ep', 'tp')), may hold values from -6 to 6
- norm_gain: float32 [2048], replicated, may hold values from 0.1 to 1.9
- gate_weight: bfloat16 [16, 2048, 2048], P('ep', None, 'tp'), may hold values from -0.375 to 0.375
- up_weight: bfloat16 [16, 2048, 2048], P('ep', None, 'tp'), may hold values from -0.375 to 0.375
- down_weight: bfloat16 [16, 2048, 2048], P('ep', 'tp'), may hold values from -0.015625 to 0.015625
- expert_choice: int32 [3072, 2], P(('ep', 'tp')), may hold values from 0 to 15, all different within a row; in each aligned block of 96 rows (0 to 95, 96 to 191, ...) at most 13 rows name the same one
- route_weights: float32 [3072, 2], P(('ep', 'tp')), may hold values from 0.2 to 1
Outputs:
- mixer_output: bfloat16 [2048, 2048], P(('ep', 'tp'))
- expert_output: bfloat16 [3072, 2048], P(('ep', 'tp'))
Inputs may be any that keep to these rules, and one draw needn't show every extreme that they name: `cumulative_gate`: each head's values never rise from one position to the next. `expert_choice`: each row names 2 different experts; within the rows of one device no expert is named more than 13 times, and in some of them one expert exactly 13 times.
All inputs are finite; a program needn't handle non-finite values.
Results may differ from a plain program's by a relative error of at most 0.019.
Values may be sent and summed in bfloat16 or wider, within the bound.
A program may use at most 128 MiB of HBM per device.

v0:
```python
import math

import jax
import jax.numpy as jnp
from jax import lax
from jax.sharding import PartitionSpec as P

EXPERTS = 16
CAP = 13


eps_norm = 1e-05
clamp_limit = 7.0
sig_alpha = 1.702
floor_score = -1e30


def attend_shard(
    carried, queries, query_gates, query_pos, key_rows, value_rows, key_gates, key_start
):
    running_max, running_sum, accum = carried
    heads_here = query_gates.shape[1]
    head_width = queries.shape[1] // heads_here
    score_scale = 1.0 / math.sqrt(head_width)
    key_pos = key_start + jnp.arange(key_rows.shape[0], dtype=jnp.int32)
    causal = key_pos[None, :] <= query_pos[:, None]
    maxima = []
    totals = []
    blocks = []
    for head_index in range(heads_here):
        first_column = head_index * head_width
        last_column = first_column + head_width
        scores = (
            jnp.einsum(
                "qd,kd->qk",
                queries[:, first_column:last_column],
                key_rows[:, first_column:last_column],
                preferred_element_type=jnp.float32,
            )
            * score_scale
        )
        scores = (
            scores + query_gates[:, head_index : head_index + 1] - key_gates[:, head_index][None, :]
        )
        scores = jnp.where(causal, scores, floor_score)
        new_peak = jnp.maximum(running_max[head_index], jnp.max(scores, axis=1))
        weights = jnp.where(causal, jnp.exp(scores - new_peak[:, None]), 0.0)
        shrink = jnp.exp(running_max[head_index] - new_peak)
        maxima.append(new_peak)
        totals.append(running_sum[head_index] * shrink + jnp.sum(weights, axis=1))
        blocks.append(
            accum[:, first_column:last_column] * shrink[:, None]
            + jnp.dot(
                weights.astype(jnp.bfloat16),
                value_rows[:, first_column:last_column],
                preferred_element_type=jnp.float32,
            )
        )
    return (jnp.stack(maxima), jnp.stack(totals), jnp.concatenate(blocks, axis=1))


def head_term(attention, out_weight):
    return jnp.dot(attention, out_weight, preferred_element_type=jnp.float32)


def expert_term(activation, down_weight, row_count):
    local_experts = down_weight.shape[0]
    grouped = activation.reshape(-1, local_experts, CAP, activation.shape[1])
    summed = jnp.einsum("neci,eid->necd", grouped, down_weight, preferred_element_type=jnp.float32)
    return summed.reshape(row_count, down_weight.shape[2])


def local(
    queries,
    key_vectors,
    value_vectors,
    cumulative_gate,
    out_weight,
    expert_tokens,
    norm_gain,
    gate_weight,
    up_weight,
    down_weight,
    expert_choice,
    route_weights,
):
    tokens_float = expert_tokens.astype(jnp.float32)
    normed = (
        tokens_float
        * lax.rsqrt(jnp.mean(tokens_float * tokens_float, axis=1, keepdims=True) + eps_norm)
        * norm_gain
    ).astype(jnp.bfloat16)
    flat_ids = expert_choice.reshape(-1)
    one_hot = (flat_ids[:, None] == jnp.arange(EXPERTS, dtype=jnp.int32)[None, :]).astype(jnp.int32)
    slot_rank = jnp.sum((jnp.cumsum(one_hot, axis=0) - one_hot) * one_hot, axis=1)
    slot_ids = (flat_ids * CAP + slot_rank).reshape(expert_tokens.shape[0], -1)
    slot_table = (
        slot_ids[:, :, None] == jnp.arange(EXPERTS * CAP, dtype=jnp.int32)[None, None, :]
    ).astype(jnp.bfloat16)
    placing = jnp.sum(slot_table, axis=1)
    outgoing = jnp.einsum("ts,td->sd", placing, normed, preferred_element_type=jnp.float32).astype(
        jnp.bfloat16
    )
    arrived = lax.all_to_all(outgoing, "ep", split_axis=0, concat_axis=0, tiled=True)
    local_experts = gate_weight.shape[0]
    row_piece = lax.all_gather(arrived, "tp", axis=0, tiled=True)
    grouped = row_piece.reshape(-1, local_experts, CAP, row_piece.shape[1])
    gate_pre = jnp.minimum(
        jnp.einsum("necd,edf->necf", grouped, gate_weight, preferred_element_type=jnp.float32),
        clamp_limit,
    )
    up_pre = jnp.clip(
        jnp.einsum("necd,edf->necf", grouped, up_weight, preferred_element_type=jnp.float32),
        -clamp_limit,
        clamp_limit,
    )
    expand_activation = (gate_pre * jax.nn.sigmoid(sig_alpha * gate_pre) * (up_pre + 1.0)).astype(
        jnp.bfloat16
    )
    activation = expand_activation.reshape(row_piece.shape[0], -1)
    slot_rows = arrived.shape[0]
    block_rows = queries.shape[0]
    heads_here = cumulative_gate.shape[1]
    first_query = lax.axis_index("ep") * block_rows
    query_pos = first_query + jnp.arange(block_rows, dtype=jnp.int32)
    last_query = first_query + block_rows - 1
    start_state = (
        jnp.full((heads_here, block_rows), floor_score, jnp.float32),
        jnp.zeros((heads_here, block_rows), jnp.float32),
        jnp.zeros((block_rows, queries.shape[1]), jnp.float32),
    )
    carried = start_state
    key_rows = lax.all_gather(key_vectors.astype(jnp.float32), "ep", axis=0, tiled=True)
    value_rows = lax.all_gather(value_vectors.astype(jnp.float32), "ep", axis=0, tiled=True)
    gate_rows = lax.all_gather(cumulative_gate, "ep", axis=0, tiled=True)
    partition_count = key_rows.shape[0] // block_rows

    def one_shard(inner_state, shard_index):
        offset = shard_index * block_rows
        shard_keys = lax.dynamic_slice_in_dim(key_rows, offset, block_rows, 0).astype(jnp.bfloat16)
        shard_values = lax.dynamic_slice_in_dim(value_rows, offset, block_rows, 0).astype(
            jnp.bfloat16
        )
        shard_gates = lax.dynamic_slice_in_dim(gate_rows, offset, block_rows, 0)
        updated = lax.cond(
            offset <= last_query,
            lambda held_state: attend_shard(
                held_state,
                queries,
                cumulative_gate,
                query_pos,
                shard_keys,
                shard_values,
                shard_gates,
                offset,
            ),
            lambda held_state: held_state,
            inner_state,
        )
        return (updated, None)

    carried, unused = lax.scan(one_shard, carried, jnp.arange(partition_count, dtype=jnp.int32))
    final_peak, final_sum, final_accum = carried
    attention = (
        (final_accum.reshape(block_rows, heads_here, -1) / final_sum.T[:, :, None])
        .reshape(block_rows, -1)
        .astype(jnp.bfloat16)
    )
    mixer_output = lax.psum_scatter(
        head_term(attention, out_weight).astype(jnp.bfloat16), "tp", scatter_dimension=0, tiled=True
    )
    slot_results = lax.psum_scatter(
        expert_term(activation, down_weight, slot_rows * lax.axis_size("tp")).astype(jnp.bfloat16),
        "tp",
        scatter_dimension=0,
        tiled=True,
    )
    returned = lax.all_to_all(slot_results, "ep", split_axis=0, concat_axis=0, tiled=True)
    picked = (
        jnp.take(returned, slot_ids.reshape(-1), axis=0)
        .astype(jnp.float32)
        .reshape(slot_ids.shape[0], slot_ids.shape[1], -1)
    )
    expert_output = jnp.sum(picked * route_weights[:, :, None], axis=1).astype(jnp.bfloat16)
    return (mixer_output, expert_output)


def solution(mesh):
    placed = (
        P("ep", "tp"),
        P("ep", "tp"),
        P("ep", "tp"),
        P("ep", "tp"),
        P("tp", None),
        P(("ep", "tp"), None),
        P(),
        P("ep", None, "tp"),
        P("ep", None, "tp"),
        P("ep", "tp", None),
        P(("ep", "tp"), None),
        P(("ep", "tp"), None),
    )
    return jax.shard_map(
        local,
        mesh=mesh,
        in_specs=placed,
        out_specs=(P(("ep", "tp"), None), P(("ep", "tp"), None)),
        check_vma=False,
    )
```

profile of v0, /device:TPU:0, one launch (start us, length us, event | category | flops | bytes accessed | tf_op | source)
XLA Modules:
  0.0 272.0 jit_solution(11689054164543764206)
XLA Ops:
  7.2 0.0 copy-start
  7.2 0.0 all-gather.2.cloned.1.call-start
  7.2 0.8 copy.33
  8.1 0.1 reshape.149
  8.2 0.6 reduce-window.6
  8.8 0.2 slice_reduce_fusion
  9.0 0.1 bitcast_bitcast_fusion
  9.1 0.1 reduce_sum.68
  9.3 0.1 copy.36
  9.3 0.7 compare_and_fusion
  10.1 0.1 fusion.61
  10.2 1.2 fusion.53
  11.3 1.5 convolution_convert_fusion.1
  12.8 0.2 all_to_all.16
  13.0 17.7 %all_to_all.24 = bf16[4,52,2048]{2,1,0:T(8,128)(2,1)S(1)} all-to-all(bf16[4,52,2048]{2,1,0:T(8,128)(2,1)S(1)} %all_to_all.16), channel_id=1, replica_groups=mesh['ep'=4,'tp'=8] {'ep'}, dimensions={0} | all-to-all | bytes 1703936 | tf_op jit(solution)/shard_map/all_to_all | solution.py:104
  30.7 1.1 all_to_all.18
  31.8 0.0 all-gather.2.cloned.1.call-update
  31.8 0.0 reduce-scatter.5.cloned.1.call-start
  31.9 68.8 %all-gather.2.cloned.1.call-done = bf16[1664,2048]{1,0:T(8,128)(2,1)} async-done(((bf16[208,2048]{1,0:T(8,128)(2,1)}), bf16[1664,2048]{1,0:T(8,128)(2,1)}) %all-gather.2.cloned.1.call-update) | async-done | bytes 6815760 | tf_op jit(solution)/shard_map/all_gather | solution.py:106
  100.7 9.1 %reshape.152 = bf16[32,4,13,2048]{3,2,1,0:T(8,128)(2,1)} reshape(bf16[1664,2048]{1,0:T(8,128)(2,1)} %all-gather.2.cloned.1.call-done) | data formatting | bytes 13631488 | tf_op jit(solution)/shard_map/reshape | solution.py:107
  109.8 9.5 %fusion.30 = f32[4,32,13,256]{3,1,2,0:T(8,128)S(1)} fusion(bf16[32,4,13,2048]{3,2,1,0:T(8,128)(2,1)} %reshape.152, bf16[4,2048,256]{2,1,0:T(8,128)(2,1)} %param.23), kind=kOutput, calls=%fused_computation.51 | convolution fusion | flops 1744830464 | bytes 12713984 | tf_op jit(solution)/shard_map/necd,edf->necf/dot_general | solution.py:109
  119.3 15.9 %convert_bitcast_fusion = bf16[32,4,13,2048]{3,0,2,1:T(8,128)(2,1)} fusion(bf16[4,256,2048]{2,1,0:T(8,128)(2,1)} %param.25, f32[4,32,13,256]{3,1,2,0:T(8,128)S(1)} %fusion.30, bf16[4,2048,256]{2,1,0:T(8,128)(2,1)} %param.24, bf16[32,4,13,2048]{3,2,1,0:T(8,128)(2,1)} %reshape.152), kind=kOutput, calls=%fused_computation.48 | convolution fusion | flops 3497328640 | bytes 23724032 | tf_op jit(solution)/shard_map/neci,eid->necd/dot_general | solution.py:69
  135.2 10.2 %copy.40 = bf16[32,4,13,2048]{3,2,1,0:T(8,128)(2,1)} copy(bf16[32,4,13,2048]{3,0,2,1:T(8,128)(2,1)} %convert_bitcast_fusion) | data formatting | bytes 13631488 | tf_op jit(solution)/shard_map/convert_element_type | solution.py:173
  145.4 9.3 %convert_element_type.78 = bf16[1664,2048]{1,0:T(8,128)(2,1)} reshape(bf16[32,4,13,2048]{3,2,1,0:T(8,128)(2,1)} %copy.40) | data formatting | bytes 13631488 | tf_op jit(solution)/shard_map/convert_element_type | solution.py:173
  154.6 0.0 reduce-scatter.5.cloned.1.call-update
  154.7 0.0 reduce-scatter.3.cloned.1.call-start
  154.7 0.6 copy-done.1
  155.3 8.1 %all_gather.14 = f32[2048,2]{0,1:T(2,128)S(1)} all-gather(f32[512,2]{0,1:T(2,128)S(1)} %copy-done.1), channel_id=1, replica_groups=mesh['ep'=4,'tp'=8] {'ep'}, dimensions={0}, use_global_device_ids=true | all-gather | bytes 20480 | tf_op jit(solution)/shard_map/all_gather | solution.py:135
  163.5 0.0 copy-done.2
  163.5 10.7 %all_gather.12 = bf16[2048,128]{1,0:T(8,128)(2,1)S(1)} all-gather(bf16[512,128]{1,0:T(8,128)(2,1)S(1)} %copy-done.2), channel_id=1, replica_groups=mesh['ep'=4,'tp'=8] {'ep'}, dimensions={0}, use_global_device_ids=true | all-gather | bytes 655360 | tf_op jit(solution)/shard_map/all_gather | solution.py:133
  174.1 0.0 copy-done.3
  174.2 9.3 %all_gather.13 = bf16[2048,128]{1,0:T(8,128)(2,1)S(1)} all-gather(bf16[512,128]{1,0:T(8,128)(2,1)S(1)} %copy-done.3), channel_id=1, replica_groups=mesh['ep'=4,'tp'=8] {'ep'}, dimensions={0}, use_global_device_ids=true | all-gather | bytes 655360 | tf_op jit(solution)/shard_map/all_gather | solution.py:134
  183.5 0.0 copy-done.6
  183.5 7.8 %while.15 = (s32[]{:T(128)}, f32[2,512]{1,0:T(2,128)S(1)}, f32[2,512]{1,0:T(2,128)S(1)}, f32[512,128]{0,1:T(8,128)S(1)}, s32[4]{0:T(128)S(1)}, /*index=5*/s32[]{...) while((s32[]{:T(128)}, f32[2,512]{1,0:T(2,128)S(1)}, ...), condition=%wide.region_7.8_spmd.clone, body=%wide.region_0.7_spmd.clone.sunk | while | flops 141499392 | bytes 8790421 | solution.py:162
  183.5 0.7 dynamic_slice.24
  184.8 2.3 conditional.3
  184.9 0.1 fusion.70
  185.0 0.4 fusion.73
  185.4 0.3 convolution_add_fusion.1
  185.7 0.5 fusion.74
  186.2 0.4 convolution_add_fusion
  186.6 0.4 fusion.7
  187.1 0.7 dynamic_slice.24
  188.5 0.7 dynamic_slice.24
  189.9 0.7 dynamic_slice.24
  191.3 0.0 copy-done
  191.3 0.0 copy-start.4
  191.3 0.0 copy-start.5
  191.3 2.1 convolution_convert_fusion
  193.4 0.0 reduce-scatter.3.cloned.1.call-update
  193.5 34.7 %reduce-scatter.5.cloned.1.call-done = bf16[208,2048]{1,0:T(8,128)(2,1)} async-done(((bf16[1664,2048]{1,0:T(8,128)(2,1)}), bf16[208,2048]{1,0:T(8,128)(2,1)}) %reduce-scatter.5.cloned.1.call-update) | async-done | bytes 851984 | tf_op jit(solution)/shard_map/reduce_scatter | solution.py:172
  228.1 2.2 all_to_all.19
  230.4 3.7 %all-to-all-start.1 = ((bf16[4,52,2048]{2,1,0:T(8,128)(2,1)}), bf16[4,52,2048]{2,1,0:T(8,128)(2,1)S(1)}, u32[]{:S(2)}, u32[]{:S(2)}) async-start(bf16[4,52,2048]{2,1,0:T(8,128)(2,1)} %all_to_all.19), calls=%async_computation.3 | async-start | bytes 1835008 | tf_op jit(solution)/shard_map/all_to_all | solution.py:178
  234.0 0.0 copy-done.4
  234.0 0.1 copy.41
  234.1 0.1 mul.123
  234.3 0.1 copy.37
  234.4 0.1 copy.42
  234.5 10.0 %all-to-all-done.1 = bf16[4,52,2048]{2,1,0:T(8,128)(2,1)S(1)} async-done(((bf16[4,52,2048]{2,1,0:T(8,128)(2,1)}), bf16[4,52,2048]{2,1,0:T(8,128)(2,1)S(1)}, u32[]{:S(2)}, u32[]{:S(2)}) %all-to-all-start.1) | async-done | bytes 852000 | tf_op jit(solution)/shard_map/all_to_all | solution.py:178
  244.5 0.2 all_to_all.21
  244.6 1.1 gather_fusion
  245.8 0.5 gather.7
  246.3 4.0 %multiply_reduce_fusion = bf16[96,2048]{1,0:T(8,128)(2,1)} fusion(bf16[96,2,2048]{2,1,0:T(2,128)(2,1)S(1)} %gather.7, pred[96,2]{1,0:T(8,128)(4,1)S(1)} %copy.37, f32[96,2]{1,0:T(8,128)S(1)} %copy.42), kind=kLoop, calls=%fused_computation.66 | loop fusion | flops 1376256 | bytes 1180608 | tf_op jit(solution)/shard_map/reduce_sum | solution.py:184
  250.3 15.2 %reduce-scatter.3.cloned.1.call-done = bf16[64,2048]{1,0:T(8,128)(2,1)} async-done(((bf16[512,2048]{1,0:T(8,128)(2,1)}), bf16[64,2048]{1,0:T(8,128)(2,1)}) %reduce-scatter.3.cloned.1.call-update) | async-done | bytes 262160 | tf_op jit(solution)/shard_map/reduce_scatter | solution.py:169
  (38 shorter events, 0.4 us)
Async XLA Ops:
  7.2 184.1 %copy-start = (bf16[128,2048]{1,0:T(8,128)(2,1)S(1)}, bf16[128,2048]{1,0:T(8,128)(2,1)}, u32[]{:S(2)}) copy-start(bf16[128,2048]{1,0:T(8,128)(2,1)} %param.20) | copy-start | bytes 1572868
  7.2 93.5 %all-gather.2.cloned.1.call-start = ((), (), s32[]{:S(2)}) async-start(), calls=%async_computation.5 | async-start | bytes 7667712 | tf_op jit(solution)/shard_map/all_gather | solution.py:106
  31.8 196.3 %reduce-scatter.5.cloned.1.call-start = ((), (), s32[]{:S(2)}) async-start(), calls=%async_computation.6 | async-start | bytes 7667712 | tf_op jit(solution)/shard_map/reduce_scatter | solution.py:172
  154.6 0.7 copy-start.1
  154.6 8.8 %copy-start.2 = (bf16[512,128]{1,0:T(8,128)(2,1)S(1)}, bf16[512,128]{1,0:T(8,128)(2,1)}, u32[]{:S(2)}) copy-start(bf16[512,128]{1,0:T(8,128)(2,1)} %param.17) | copy-start | bytes 393220
  154.6 19.5 %copy-start.3 = (bf16[512,128]{1,0:T(8,128)(2,1)S(1)}, bf16[512,128]{1,0:T(8,128)(2,1)}, u32[]{:S(2)}) copy-start(bf16[512,128]{1,0:T(8,128)(2,1)} %param.18) | copy-start | bytes 393220
  154.6 28.8 %copy-start.6 = (bf16[512,128]{1,0:T(8,128)(2,1)S(1)}, bf16[512,128]{1,0:T(8,128)(2,1)}, u32[]{:S(2)}) copy-start(bf16[512,128]{1,0:T(8,128)(2,1)} %param.16) | copy-start | bytes 393220
  154.7 110.8 %reduce-scatter.3.cloned.1.call-start = ((), (), s32[]{:S(2)}) async-start(), calls=%async_computation.4 | async-start | bytes 2359296 | tf_op jit(solution)/shard_map/reduce_scatter | solution.py:169
  191.3 42.7 %copy-start.4 = (s32[96,2]{0,1:T(2,128)S(1)}, s32[96,2]{0,1:T(2,128)}, u32[]{:S(2)}) copy-start(s32[96,2]{0,1:T(2,128)} %param.26) | copy-start | bytes 2308
  191.3 43.1 %copy-start.5 = (f32[96,2]{0,1:T(2,128)S(1)}, f32[96,2]{0,1:T(2,128)}, u32[]{:S(2)}) copy-start(f32[96,2]{0,1:T(2,128)} %param.27) | copy-start | bytes 2308
  230.4 14.1 %all-to-all-start.1 = ((bf16[4,52,2048]{2,1,0:T(8,128)(2,1)}), bf16[4,52,2048]{2,1,0:T(8,128)(2,1)S(1)}, u32[]{:S(2)}, u32[]{:S(2)}) async-start(bf16[4,52,2048]{2,1,0:T(8,128)(2,1)} %all_to_all.19), calls=%async_computation.3 | async-start | bytes 1835008 | tf_op jit(solution)/shard_map/all_to_all | solution.py:178
Sparse Core Ops, SparseCore 0:
  31.9 68.7 all-gather.1
  154.8 73.2 reduce-scatter.4
  231.0 34.4 reduce-scatter.2
where the time goes:
time: 273 us; the launch traced here: 272 us
  waiting for transfers between devices  129 us (47%)
  blocking collectives  45.8 us (17%)
  local copies, waits for them, and re-layouts  39.1 us (14%)
  matrix products  30.6 us (11%)
  between operations  13.9 us (5%)
  other arithmetic  7.29 us (3%)
  starting transfers between devices  3.77 us (1%)
  loops' own time  2.88 us (1%)
    all_gather x1, waiting for transfers between devices, local(): row_piece = lax.all_gather(arrived, 'tp', axis=0, tiled=True)  68.8 us
    reduce_scatter x1, waiting for transfers between devices, local(): lax.psum_scatter(expert_term(activation, down_weight, slot_rows * lax.axi...  34.7 us
    convert_element_type x2, local copies, waits for them, and re-layouts, local(): expert_term(activation, down_weight, slot_rows * lax.axis_size('tp'))  19.4 us
    all_to_all x1, blocking collectives, local(): lax.all_to_all(outgoing, 'ep', split_axis=0, concat_axis=0, tiled=True)  17.7 us
    dot_general x1, matrix products, expert_term(): jnp.einsum('neci,eid->necd', grouped, down_weight, preferred_element_type...  15.9 us
    reduce_scatter x1, waiting for transfers between devices, local(): lax.psum_scatter(head_term(attention, out_weight).astype(jnp.bfloat16), '...  15.2 us
    all_gather x1, blocking collectives, local(): lax.all_gather(key_vectors.astype(jnp.float32), 'ep', axis=0, tiled=True)  10.7 us
    all_to_all x1, waiting for transfers between devices, local(): lax.all_to_all(slot_results, 'ep', split_axis=0, concat_axis=0, tiled=True)  9.95 us
  transfers between devices with their start and end apart: 4, of which 4 were waited for; matrix products, arithmetic and copies ran while one was open for 5% of the time, Pallas kernels for 0%

commit v1 on v0

v1 whole, which is shorter than its diff:
```python
import functools
import math

import jax
import jax.numpy as jnp
from jax import lax
from jax.experimental import pallas as pl
from jax.experimental.pallas import tpu as pltpu
from jax.sharding import PartitionSpec as P

SLOTS = 16
CORES = 2
MESH = pl.DeviceIdType.MESH


eps_norm = 1e-05
clamp_limit = 7.0
sig_alpha = 1.702
floor_score = -1e30


def attend_shard(
    carried, queries, query_gates, query_pos, key_rows, value_rows, key_gates, key_start
):
    running_max, running_sum, accum = carried
    heads_here = query_gates.shape[1]
    head_width = queries.shape[1] // heads_here
    score_scale = 1.0 / math.sqrt(head_width)
    key_pos = key_start + jnp.arange(key_rows.shape[0], dtype=jnp.int32)
    causal = key_pos[None, :] <= query_pos[:, None]
    maxima = []
    totals = []
    blocks = []
    for head_index in range(heads_here):
        first_column = head_index * head_width
        last_column = first_column + head_width
        scores = (
            jnp.einsum(
                "qd,kd->qk",
                queries[:, first_column:last_column],
                key_rows[:, first_column:last_column],
                preferred_element_type=jnp.float32,
            )
            * score_scale
        )
        scores = (
            scores + query_gates[:, head_index : head_index + 1] - key_gates[:, head_index][None, :]
        )
        scores = jnp.where(causal, scores, floor_score)
        new_peak = jnp.maximum(running_max[head_index], jnp.max(scores, axis=1))
        weights = jnp.where(causal, jnp.exp(scores - new_peak[:, None]), 0.0)
        shrink = jnp.exp(running_max[head_index] - new_peak)
        maxima.append(new_peak)
        totals.append(running_sum[head_index] * shrink + jnp.sum(weights, axis=1))
        blocks.append(
            accum[:, first_column:last_column] * shrink[:, None]
            + jnp.dot(
                weights.astype(jnp.bfloat16),
                value_rows[:, first_column:last_column],
                preferred_element_type=jnp.float32,
            )
        )
    return (jnp.stack(maxima), jnp.stack(totals), jnp.concatenate(blocks, axis=1))


def head_term(attention, out_weight):
    return jnp.dot(attention, out_weight, preferred_element_type=jnp.float32)


def greet(e, t, ep, nz):
    z, c = t // CORES, t % CORES
    barrier = pltpu.get_barrier_semaphore()
    peers = [(e, z * CORES + 1 - c)]
    peers += [(e, lax.rem(z + k, nz) * CORES + c) for k in range(1, nz)]
    peers += [(lax.rem(e + j, ep), t) for j in range(1, ep)]
    for peer in peers:
        pl.semaphore_signal(barrier, inc=1, device_id=peer, device_id_type=MESH)
    pl.semaphore_wait(barrier, len(peers))


def dispatch_kernel(
    ep, nz, local_experts, x_ref, meta_ref, out_ref, metas_ref, xbuf, outbox,
    xs, xr, ms, mr, cs, cr, ds, dr,
):
    e, t = lax.axis_index("ep"), lax.axis_index("tp")
    z, c = t // CORES, t % CORES
    partner = (e, z * CORES + 1 - c)
    rows = x_ref.shape[0]
    greet(e, t, ep, nz)

    def token_copy(k):
        dest = (e, lax.rem(z + k, nz) * CORES + c)
        return (
            pltpu.make_async_remote_copy(
                src_ref=meta_ref, dst_ref=metas_ref.at[k], send_sem=ms.at[k], recv_sem=mr.at[k],
                device_id=dest, device_id_type=MESH,
            ),
            pltpu.make_async_remote_copy(
                src_ref=x_ref, dst_ref=xbuf.at[k], send_sem=xs.at[k], recv_sem=xr.at[k],
                device_id=dest, device_id_type=MESH,
            ),
        )

    def origin(k):
        return lax.rem(z - k + nz, nz)

    def row_copy(k, j):
        return pltpu.make_async_remote_copy(
            src_ref=outbox.at[k, lax.rem(e + j, ep)], dst_ref=out_ref.at[:, c, e, origin(k)],
            send_sem=cs.at[k, j], recv_sem=cr.at[k, j],
            device_id=(lax.rem(e + j, ep), t), device_id_type=MESH,
        )

    def share_copy(k, j):
        source = out_ref.at[:, c, lax.rem(e - j + ep, ep), origin(k)]
        return pltpu.make_async_remote_copy(
            src_ref=source, dst_ref=source, send_sem=ds.at[k, j], recv_sem=dr.at[k, j],
            device_id=partner, device_id_type=MESH,
        )

    order = sorted(range(1, nz), key=lambda k: min(k, nz - k))
    for k in order:
        for copy in token_copy(k):
            copy.start()
    far_first = [2] + [j for j in range(1, ep) if j != 2] if ep > 2 else list(range(1, ep))
    metas_ref[0] = meta_ref[...]
    for n, k in enumerate([0] + order):
        if k > 0:
            for copy in token_copy(k):
                copy.wait_recv()
        block = x_ref if k == 0 else xbuf.at[k]
        info = metas_ref[k]
        slot = lax.broadcasted_iota(jnp.int32, (ep * local_experts * SLOTS, rows), 0).astype(
            jnp.float32
        )
        chosen = (slot == info[0:1, :rows]) | (slot == info[1:2, :rows])
        picked = jnp.dot(
            jnp.where(chosen, 1.0, 0.0).astype(jnp.bfloat16), block[...],
            preferred_element_type=jnp.float32,
        ).astype(jnp.bfloat16)
        outbox[k] = picked.reshape(ep, local_experts, SLOTS, picked.shape[1])
        for j in far_first:
            row_copy(k, j).start()
        out_ref[:, c, e, origin(k)] = outbox[k, e]
        share_copy(k, 0).start()
    for k in [0] + order:
        for j in range(1, ep):
            row_copy(k, j).wait_recv()
            share_copy(k, j).start()
    for k in range(nz):
        for j in range(ep):
            share_copy(k, j).wait_send()
            other = out_ref.at[:, 1 - c, lax.rem(e - j + ep, ep), origin(k)]
            pltpu.make_async_remote_copy(
                src_ref=other, dst_ref=other, send_sem=ds.at[k, j], recv_sem=dr.at[k, j],
                device_id=partner, device_id_type=MESH,
            ).wait_recv()
            if j > 0:
                row_copy(k, j).wait_send()
        if k > 0:
            for copy in token_copy(k):
                copy.wait_send()


def dispatch(x, meta, ep, nz, local_experts):
    width = x.shape[1]
    dma = pltpu.SemaphoreType.DMA
    return pl.pallas_call(
        functools.partial(dispatch_kernel, ep, nz, local_experts),
        out_shape=(
            jax.ShapeDtypeStruct((local_experts, CORES, ep, nz, SLOTS, width), jnp.bfloat16),
            jax.ShapeDtypeStruct((nz,) + meta.shape, jnp.float32),
        ),
        in_specs=[pl.BlockSpec(memory_space=pltpu.VMEM)] * 2,
        out_specs=[pl.BlockSpec(memory_space=pltpu.VMEM)] * 2,
        scratch_shapes=[
            pltpu.VMEM((nz,) + x.shape, jnp.bfloat16),
            pltpu.VMEM((nz, ep, local_experts, SLOTS, width), jnp.bfloat16),
            dma((nz,)), dma((nz,)), dma((nz,)), dma((nz,)),
            dma((nz, ep)), dma((nz, ep)), dma((nz, ep)), dma((nz, ep)),
        ],
        compiler_params=pltpu.CompilerParams(
            collective_id=0, has_side_effects=True, vmem_limit_bytes=60 * 1024 * 1024
        ),
        cost_estimate=pl.CostEstimate(
            flops=30_000_000_000, bytes_accessed=20_000_000, transcendentals=0
        ),
    )(x, meta)


def combine_kernel(
    ep, nz, local_experts, part_ref, metas_ref, out_ref, pair, sums, rows_in, outbox, final,
    ps, pr, cs, cr, fs, fr,
):
    e, t = lax.axis_index("ep"), lax.axis_index("tp")
    z, c = t // CORES, t % CORES
    partner = (e, z * CORES + 1 - c)
    tokens = out_ref.shape[0]
    width = out_ref.shape[1]
    greet(e, t, ep, nz)
    group = local_experts * SLOTS

    def column(j):
        return lax.rem(e + j, ep)

    def target(k):
        return lax.rem(z - k + nz, nz)

    def pair_copy(k, j):
        return pltpu.make_async_remote_copy(
            src_ref=part_ref.at[:, 1 - c, column(j), target(k)], dst_ref=pair.at[k, j],
            send_sem=ps.at[k, j], recv_sem=pr.at[k, j], device_id=partner, device_id_type=MESH,
        )

    def row_copy(k, j):
        return pltpu.make_async_remote_copy(
            src_ref=sums.at[k, j], dst_ref=rows_in.at[k, j],
            send_sem=cs.at[k, j], recv_sem=cr.at[k, j],
            device_id=(column(j), t), device_id_type=MESH,
        )

    def final_copy(k):
        return pltpu.make_async_remote_copy(
            src_ref=outbox.at[k], dst_ref=final.at[k], send_sem=fs.at[k], recv_sem=fr.at[k],
            device_id=(e, target(k) * CORES + c), device_id_type=MESH,
        )

    far_first = [2] + [j for j in range(1, ep) if j != 2] if ep > 2 else list(range(1, ep))
    order = sorted(range(1, nz), key=lambda k: -min(k, nz - k)) + [0]
    for k in order:
        for j in far_first + [0]:
            pair_copy(k, j).start()

    def add_pairs(k):
        for j in far_first + [0]:
            pair_copy(k, j).wait_recv()
            sums[k, j] = (
                part_ref[:, c, column(j), target(k)].astype(jnp.float32)
                + pair[k, j].astype(jnp.float32)
            ).astype(jnp.bfloat16)
            if j > 0:
                row_copy(k, j).start()

    def combine(k):
        info = metas_ref[k]
        total = jnp.zeros((tokens, width), jnp.float32)
        for j in range(ep):
            if j > 0:
                row_copy(k, j).wait_recv()
            held = (sums if j == 0 else rows_in)[k, j].reshape(group, width)
            first = (lax.rem(e - j + ep, ep) * group).astype(jnp.float32)
            slot = first + lax.broadcasted_iota(jnp.int32, (group, tokens), 0).astype(jnp.float32)
            weight = jnp.where(slot == info[0:1, :tokens], info[2:3, :tokens], 0.0) + jnp.where(
                slot == info[1:2, :tokens], info[3:4, :tokens], 0.0
            )
            high = weight.astype(jnp.bfloat16)
            low = (weight - high.astype(jnp.float32)).astype(jnp.bfloat16)
            for piece in (high, low):
                total = total + lax.dot_general(
                    piece, held, (((0,), (0,)), ((), ())), preferred_element_type=jnp.float32
                )
        return total

    for k in order:
        add_pairs(k)
    for k in order[:-1]:
        outbox[k] = combine(k).astype(jnp.bfloat16)
        final_copy(k).start()
    total = combine(0)
    for k in order[:-1]:
        final_copy(k).wait_recv()
        total = total + final[k].astype(jnp.float32)
    out_ref[...] = total.astype(jnp.bfloat16)
    for k in range(nz):
        if k > 0:
            final_copy(k).wait_send()
        for j in range(ep):
            pair_copy(k, j).wait_send()
            if j > 0:
                row_copy(k, j).wait_send()


def combine_rows(part, metas, tokens, ep, nz, local_experts):
    width = part.shape[-1]
    dma = pltpu.SemaphoreType.DMA
    box = (nz, ep, local_experts, SLOTS, width)
    return pl.pallas_call(
        functools.partial(combine_kernel, ep, nz, local_experts),
        out_shape=jax.ShapeDtypeStruct((tokens, width), jnp.bfloat16),
        in_specs=[pl.BlockSpec(memory_space=pltpu.VMEM)] * 2,
        out_specs=pl.BlockSpec(memory_space=pltpu.VMEM),
        scratch_shapes=[
            pltpu.VMEM(box, jnp.bfloat16),
            pltpu.VMEM(box, jnp.bfloat16),
            pltpu.VMEM(box, jnp.bfloat16),
            pltpu.VMEM((nz, tokens, width), jnp.bfloat16),
            pltpu.VMEM((nz, tokens, width), jnp.bfloat16),
            dma((nz, ep)), dma((nz, ep)), dma((nz, ep)), dma((nz, ep)), dma((nz,)), dma((nz,)),
        ],
        compiler_params=pltpu.CompilerParams(
            collective_id=1, has_side_effects=True, vmem_limit_bytes=60 * 1024 * 1024
        ),
        cost_estimate=pl.CostEstimate(
            flops=40_000_000_000, bytes_accessed=20_000_000, transcendentals=0
        ),
    )(part, metas)


def local(
    queries, key_vectors, value_vectors, cumulative_gate, out_weight, expert_tokens, norm_gain,
    gate_weight, up_weight, down_weight, expert_choice, route_weights,
):
    ep, nz = lax.axis_size("ep"), lax.axis_size("tp") // CORES
    tokens, width = expert_tokens.shape
    local_experts = gate_weight.shape[0]
    gate_high = lax.reduce_precision(cumulative_gate, 8, 7)
    gate_rest = cumulative_gate - gate_high
    gate_mid = lax.reduce_precision(gate_rest, 8, 7)
    gate_low = gate_rest - gate_mid
    shared = jnp.concatenate(
        [key_vectors, value_vectors]
        + [piece.astype(jnp.bfloat16) for piece in (gate_high, gate_mid, gate_low)],
        axis=1,
    )
    all_rows = lax.all_gather(shared, "ep", axis=0, tiled=True)

    tokens_float = expert_tokens.astype(jnp.float32)
    normed = (
        tokens_float
        * lax.rsqrt(jnp.mean(tokens_float * tokens_float, axis=1, keepdims=True) + eps_norm)
        * norm_gain
    ).astype(jnp.bfloat16)
    flat_ids = expert_choice.reshape(-1)
    one_hot = (flat_ids[:, None] == jnp.arange(ep * local_experts, dtype=jnp.int32)[None, :]).astype(
        jnp.float32
    )
    position = jnp.arange(flat_ids.shape[0], dtype=jnp.int32)
    earlier = (position[:, None] > position[None, :]).astype(jnp.float32)
    slot_rank = jnp.sum(jnp.dot(earlier, one_hot) * one_hot, axis=1)
    slot_ids = (flat_ids.astype(jnp.float32) * SLOTS + slot_rank).reshape(tokens, -1)
    meta = jnp.concatenate([slot_ids.T, route_weights.T], axis=0)
    meta = jnp.pad(meta, ((0, 8 - meta.shape[0]), (0, -tokens % 128)), constant_values=-1.0)
    grouped, metas = dispatch(normed, meta, ep, nz, local_experts)

    kept = queries.shape[1]
    heads_here = cumulative_gate.shape[1]
    grouped, all_rows = lax.optimization_barrier((grouped, all_rows))
    key_rows, value_rows = all_rows[:, :kept], all_rows[:, kept : 2 * kept]
    pieces = all_rows[:, 2 * kept :].astype(jnp.float32)
    gate_rows = (
        pieces[:, :heads_here] + pieces[:, heads_here : 2 * heads_here]
    ) + pieces[:, 2 * heads_here :]
    block_rows = queries.shape[0]
    first_query = lax.axis_index("ep") * block_rows
    query_pos = first_query + jnp.arange(block_rows, dtype=jnp.int32)
    last_query = first_query + block_rows - 1
    carried = (
        jnp.full((heads_here, block_rows), floor_score, jnp.float32),
        jnp.zeros((heads_here, block_rows), jnp.float32),
        jnp.zeros((block_rows, kept), jnp.float32),
    )

    def one_shard(inner_state, shard_index):
        offset = shard_index * block_rows
        shard_keys = lax.dynamic_slice_in_dim(key_rows, offset, block_rows, 0)
        shard_values = lax.dynamic_slice_in_dim(value_rows, offset, block_rows, 0)
        shard_gates = lax.dynamic_slice_in_dim(gate_rows, offset, block_rows, 0)
        updated = lax.cond(
            offset <= last_query,
            lambda held_state: attend_shard(
                held_state, queries, cumulative_gate, query_pos, shard_keys, shard_values,
                shard_gates, offset,
            ),
            lambda held_state: held_state,
            inner_state,
        )
        return (updated, None)

    carried, unused = lax.scan(one_shard, carried, jnp.arange(ep, dtype=jnp.int32))
    final_peak, final_sum, final_accum = carried
    attention = (
        (final_accum.reshape(block_rows, heads_here, -1) / final_sum.T[:, :, None])
        .reshape(block_rows, -1)
        .astype(jnp.bfloat16)
    )
    mixed = head_term(attention, out_weight).astype(jnp.bfloat16)
    grouped, mixed = lax.optimization_barrier((grouped, mixed))
    mixer_output = lax.psum_scatter(mixed, "tp", scatter_dimension=0, tiled=True)

    rows_in = grouped.reshape(local_experts, -1, width)
    gate_pre = jnp.minimum(
        jnp.einsum("ecd,edf->ecf", rows_in, gate_weight, preferred_element_type=jnp.float32),
        clamp_limit,
    )
    up_pre = jnp.clip(
        jnp.einsum("ecd,edf->ecf", rows_in, up_weight, preferred_element_type=jnp.float32),
        -clamp_limit,
        clamp_limit,
    )
    activation = (gate_pre * jax.nn.sigmoid(sig_alpha * gate_pre) * (up_pre + 1.0)).astype(
        jnp.bfloat16
    )
    part = jnp.einsum(
        "eci,eid->ecd", activation, down_weight, preferred_element_type=jnp.float32
    ).astype(jnp.bfloat16)
    expert_output = combine_rows(part.reshape(grouped.shape), metas, tokens, ep, nz, local_experts)
    return (mixer_output, expert_output)


def solution(mesh):
    placed = (
        P("ep", "tp"),
        P("ep", "tp"),
        P("ep", "tp"),
        P("ep", "tp"),
        P("tp", None),
        P(("ep", "tp"), None),
        P(),
        P("ep", None, "tp"),
        P("ep", None, "tp"),
        P("ep", "tp", None),
        P(("ep", "tp"), None),
        P(("ep", "tp"), None),
    )
    return jax.shard_map(
        local,
        mesh=mesh,
        in_specs=placed,
        out_specs=(P(("ep", "tp"), None), P(("ep", "tp"), None)),
        check_vma=False,
    )
```

time: 273 us -> 195 us (0.71)
  Pallas kernels: 0 us -> 135 us
  waiting for transfers between devices: 129 us -> 0.07 us
  blocking collectives: 45.8 us -> 0 us
  local copies, waits for them, and re-layouts: 39.1 us -> 9.52 us
  matrix products: 30.6 us -> 24.9 us
  starting transfers between devices: 3.77 us -> 0.08 us
    pallas_call x0 -> x2, Pallas kernels: none -> 135 us  [the longest x1 69.9 us: dispatch(): pl.pallas_call(functools.partial(dispatch_kernel, ep, nz, local_experts),...]
    all_gather x1, waiting for transfers between devices: 68.8 us -> 0.02 us  [local(): all_rows = lax.all_gather(shared, 'ep', axis=0, tiled=True)]
    reduce_scatter x2 -> x1, waiting for transfers between devices: 49.8 us -> 0.02 us  [local(): lax.psum_scatter(mixed, 'tp', scatter_dimension=0, tiled=True)]
    all_gather x3 -> x0, blocking collectives: 28.1 us -> none  [the longest x1 10.7 us: local(): lax.all_gather(key_vectors.astype(jnp.float32), 'ep', axis=0, tiled=True)]
    convert_element_type x6 -> x3, local copies, waits for them, and re-layouts: 19.5 us -> 0.57 us  [local(): piece.astype(jnp.bfloat16)]
    all_to_all x1 -> x0, blocking collectives: 17.7 us -> none  [local(): lax.all_to_all(outgoing, 'ep', split_axis=0, concat_axis=0, tiled=True)]
    all_to_all x1 -> x0, waiting for transfers between devices: 9.95 us -> none  [local(): lax.all_to_all(slot_results, 'ep', split_axis=0, concat_axis=0, tiled=True)]
    reshape x2 -> x0, local copies, waits for them, and re-layouts: 9.23 us -> none  [the longest x1 9.09 us: local(): grouped = row_piece.reshape(-1, local_experts, CAP, row_piece.shape[1])]
  transfers between devices with their start and end apart: 4 -> 2, of which waited for: 4 -> 0; matrix products, arithmetic and copies ran while one was open for 5% -> 14% of each run, Pallas kernels for 0% -> 69%
where the time goes in v1:
time: 195 us
  Pallas kernels  135 us (69%)
  matrix products  24.9 us (13%)
  between operations  14.2 us (7%)
  local copies, waits for them, and re-layouts  9.52 us (5%)
  other arithmetic  8.05 us (4%)
  loops' own time  3.08 us (2%)
    pallas_call x1, Pallas kernels, dispatch(): pl.pallas_call(functools.partial(dispatch_kernel, ep, nz, local_experts),...  69.9 us
    pallas_call x1, Pallas kernels, combine_rows(): pl.pallas_call(functools.partial(combine_kernel, ep, nz, local_experts),...  65 us
    dot_general x1, matrix products, local(): jnp.einsum('eci,eid->ecd', activation, down_weight, preferred_element_typ...  14.1 us
    dot_general x1, matrix products, local(): jnp.einsum('ecd,edf->ecf', rows_in, gate_weight, preferred_element_type=j...  6.9 us
  transfers between devices with their start and end apart: 2, of which 0 were waited for; matrix products, arithmetic and copies ran while one was open for 14% of the time, Pallas kernels for 69%

profile of v1, /device:TPU:0, one launch (start us, length us, event | category | flops | bytes accessed | tf_op | source)
XLA Modules:
  0.0 194.7 jit_solution(3763836257885973216)
XLA Ops:
  7.2 0.0 copy-start
  7.2 0.0 all-gather.2.cloned.1.call-start
  7.2 0.7 fusion.42
  8.0 0.2 copy.26
  8.2 0.2 copy.24
  8.4 0.2 copy.25
  8.6 1.9 concatenate.13
  10.5 0.0 all-gather.2.cloned.1.call-update
  10.5 0.0 reduce-scatter.2.cloned.1.call-start
  10.5 1.2 fusion.37
  11.7 0.8 copy.22
  12.5 0.1 eq.15
  12.7 0.2 fusion.32
  12.8 0.2 reduce_sum.50
  13.0 0.1 copy.23
  13.0 0.7 add_bitcast_fusion
  13.8 1.3 select_maximum_fusion.meta_ref
  15.0 1.9 fusion.39.x_ref
  16.9 69.9 %shard_map.131 = (bf16[4,2,4,4,16,2048]{5,4,3,2,1,0:T(8,128)(2,1)}, f32[4,8,128]{2,1,0:T(8,128)}) custom-call(bf16[96,2048]{1,0:T(8,128)(2,1)} %fusion.39.x_ref, f32[8,128]{1,0:T(8,128)} %select_maximum_fusion.meta_ref), custom_call_target="tpu_custom_call" | custom-call | flops 30000001024 | bytes 20000000 | tf_op jit(solution)/shard_map/pallas_call | solution.py:168
  86.8 0.0 all-gather.2.cloned.1.call-done
  86.8 1.1 slice_convert_fusion
  87.9 0.0 copy-start.1
  88.0 0.0 copy-start.2
  88.0 1.3 fusion.52
  89.3 0.6 slice_add_fusion
  89.9 0.3 copy.27
  90.3 0.0 copy-done.1
  90.3 0.0 copy-done.2
  90.3 7.7 %while.15 = (s32[]{:T(128)}, f32[2,512]{1,0:T(2,128)S(1)}, f32[2,512]{1,0:T(2,128)S(1)}, f32[512,128]{0,1:T(8,128)S(1)}, s32[4]{0:T(128)S(1)}, /*index=5*/s32[]{...) while((s32[]{:T(128)}, f32[2,512]{1,0:T(2,128)S(1)}, ...), condition=%wide.region_9.10_spmd.clone, body=%wide.region_2.9_spmd.clone.sunk | while | flops 141499392 | bytes 8266149 | solution.py:379
  90.3 0.6 dynamic_slice.33
  91.5 2.3 %conditional.3 = ((f32[2,512]{1,0:T(2,128)S(1)}, f32[2,512]{1,0:T(2,128)S(1)}, f32[512,128]{0,1:T(8,128)S(1)})) conditional(s32[]{:T(128)} %convert_element_type.88, (f32[2,512]{1,0:T(2,128)S(1)}, f32[2,512]{1,0:T(2,128)S(1)}, f32[512,128]{0,1:T(8,128)S(1)}) %tuple.70, (f32[2,512]{1,0:T(2,128)S(1)}, s32[]{:T(128)}, s32[]{:T(128)}, ...), branch_computations={%region_3.3_spmd, %region_4.8_spmd} | conditional | flops 141499392 | bytes 8263810 | solution.py:368
  91.6 0.1 fusion.47
  91.7 0.4 fusion.50
  92.1 0.4 convolution_add_fusion.1
  92.5 0.5 fusion.51
  92.9 0.4 fusion.9
  93.4 0.4 convolution_add_fusion
  93.9 0.6 dynamic_slice.33
  95.2 0.6 dynamic_slice.33
  96.5 0.6 dynamic_slice.33
  98.0 0.0 copy-done
  98.0 2.1 %convolution_convert_fusion.1 = bf16[512,2048]{1,0:T(8,128)(2,1)} fusion(bf16[512,128]{0,1:T(8,128)(2,1)S(1)} %fusion.40, bf16[128,2048]{1,0:T(8,128)(2,1)S(1)} %copy-done), kind=kOutput, calls=%fused_computation.50 | convolution fusion | flops 269484032 | bytes 2752512 | tf_op jit(solution)/shard_map/dot_general | solution.py:67
  100.1 0.0 reduce-scatter.2.cloned.1.call-update
  100.1 6.9 %fusion.53 = f32[4,512,256]{2,1,0:T(8,128)S(1)} fusion(bf16[4,512,2048]{2,1,0:T(8,128)(2,1)} %bitcast.50, bf16[4,2048,256]{2,1,0:T(8,128)(2,1)} %param.23), kind=kOutput, calls=%fused_computation.91 | convolution fusion | flops 2147483648 | bytes 14680064 | tf_op jit(solution)/shard_map/ecd,edf->ecf/dot_general | solution.py:392
  107.0 14.1 %convolution_convert_fusion = bf16[4,512,2048]{2,1,0:T(8,128)(2,1)} fusion(bf16[4,256,2048]{2,1,0:T(8,128)(2,1)} %param.25, f32[4,512,256]{2,1,0:T(8,128)S(1)} %fusion.53, bf16[4,512,2048]{2,1,0:T(8,128)(2,1)} %bitcast.51, bf16[4,2048,256]{2,1,0:T(8,128)(2,1)} %param.24), kind=kOutput, calls=%fused_computation.49 | convolution fusion | flops 4304404480 | bytes 27262976 | tf_op jit(solution)/shard_map/eci,eid->ecd/dot_general | solution.py:403
  121.1 65.0 %shard_map.132 = bf16[96,2048]{1,0:T(8,128)(2,1)} custom-call(bf16[4,2,4,4,16,2048]{5,4,3,2,1,0:T(8,128)(2,1)} %bitcast.52, f32[4,8,128]{2,1,0:T(8,128)} %get-tuple-element.208.metas_ref), custom_call_target="tpu_custom_call" | custom-call | flops 40000000000 | bytes 20000000 | tf_op jit(solution)/shard_map/pallas_call | solution.py:287
  186.1 0.0 reduce-scatter.2.cloned.1.call-done
  186.1 1.8 copy.49
  (21 shorter events, 0.2 us)
Async XLA Ops:
  7.2 90.8 %copy-start = (bf16[128,2048]{1,0:T(8,128)(2,1)S(1)}, bf16[128,2048]{1,0:T(8,128)(2,1)}, u32[]{:S(2)}) copy-start(bf16[128,2048]{1,0:T(8,128)(2,1)} %param.20) | copy-start | bytes 1572868
  7.2 79.6 %all-gather.2.cloned.1.call-start = ((), (), s32[]{:S(2)}) async-start(), calls=%async_computation.1 | async-start | bytes 1966080 | tf_op jit(solution)/shard_map/all_gather | solution.py:325
  10.5 175.6 %reduce-scatter.2.cloned.1.call-start = ((), (), s32[]{:S(2)}) async-start(), calls=%async_computation.2 | async-start | bytes 2359296 | tf_op jit(solution)/shard_map/reduce_scatter | solution.py:388
  87.9 2.3 %copy-start.1 = (f32[512,2]{0,1:T(2,128)S(1)}, f32[512,2]{0,1:T(2,128)}, u32[]{:S(2)}) copy-start(f32[512,2]{0,1:T(2,128)} %param.19) | copy-start | bytes 12292
  88.0 2.3 %copy-start.2 = (bf16[512,128]{1,0:T(8,128)(2,1)S(1)}, bf16[512,128]{1,0:T(8,128)(2,1)}, u32[]{:S(2)}) copy-start(bf16[512,128]{1,0:T(8,128)(2,1)} %param.16) | copy-start | bytes 393220
Sparse Core Ops, SparseCore 0:
  10.6 57.6 all-gather.1
  100.2 42.5 reduce-scatter.1

commit v2 on v1

v2 whole, which is shorter than its diff:
```python
import functools
import math

import jax
import jax.numpy as jnp
from jax import lax
from jax.experimental import pallas as pl
from jax.experimental.pallas import tpu as pltpu
from jax.sharding import PartitionSpec as P

SLOTS = 16
CORES = 2
MESH = pl.DeviceIdType.MESH


eps_norm = 1e-05
clamp_limit = 7.0
sig_alpha = 1.702
floor_score = -1e30


def attend_shard(
    carried, queries, query_gates, query_pos, key_rows, value_rows, key_gates, key_start
):
    running_max, running_sum, accum = carried
    heads_here = query_gates.shape[1]
    head_width = queries.shape[1] // heads_here
    score_scale = 1.0 / math.sqrt(head_width)
    key_pos = key_start + jnp.arange(key_rows.shape[0], dtype=jnp.int32)
    causal = key_pos[None, :] <= query_pos[:, None]
    maxima = []
    totals = []
    blocks = []
    for head_index in range(heads_here):
        first_column = head_index * head_width
        last_column = first_column + head_width
        scores = (
            jnp.einsum(
                "qd,kd->qk",
                queries[:, first_column:last_column],
                key_rows[:, first_column:last_column],
                preferred_element_type=jnp.float32,
            )
            * score_scale
        )
        scores = (
            scores + query_gates[:, head_index : head_index + 1] - key_gates[:, head_index][None, :]
        )
        scores = jnp.where(causal, scores, floor_score)
        new_peak = jnp.maximum(running_max[head_index], jnp.max(scores, axis=1))
        weights = jnp.where(causal, jnp.exp(scores - new_peak[:, None]), 0.0)
        shrink = jnp.exp(running_max[head_index] - new_peak)
        maxima.append(new_peak)
        totals.append(running_sum[head_index] * shrink + jnp.sum(weights, axis=1))
        blocks.append(
            accum[:, first_column:last_column] * shrink[:, None]
            + jnp.dot(
                weights.astype(jnp.bfloat16),
                value_rows[:, first_column:last_column],
                preferred_element_type=jnp.float32,
            )
        )
    return (jnp.stack(maxima), jnp.stack(totals), jnp.concatenate(blocks, axis=1))


def head_term(attention, out_weight):
    return jnp.dot(attention, out_weight, preferred_element_type=jnp.float32)


def greet(e, t, ep, nz):
    z, c = t // CORES, t % CORES
    barrier = pltpu.get_barrier_semaphore()
    peers = [(e, z * CORES + 1 - c)]
    peers += [(e, lax.rem(z + k, nz) * CORES + c) for k in range(1, nz)]
    peers += [(lax.rem(e + j, ep), t) for j in range(1, ep)]
    for peer in peers:
        pl.semaphore_signal(barrier, inc=1, device_id=peer, device_id_type=MESH)
    pl.semaphore_wait(barrier, len(peers))


def expert_kernel(
    ep, nz, local_experts, x_ref, meta_ref, gate_ref, up_ref, down_ref, out_ref,
    metas, xbuf, outbox, rows, pair, rows_in, finalbox, final, gate_w, up_w, down_w,
    xs, xr, ms, mr, cs, cr, ds, dr, ps, pr, bs, br, fs, fr, ws,
):
    e, t = lax.axis_index("ep"), lax.axis_index("tp")
    z, c = t // CORES, t % CORES
    partner = (e, z * CORES + 1 - c)
    tokens, width = x_ref.shape
    group = local_experts * SLOTS
    greet(e, t, ep, nz)

    def column(j):
        return lax.rem(e + j, ep)

    def behind(j):
        return lax.rem(e - j + ep, ep)

    def remote(src, dst, send, recv, device):
        return pltpu.make_async_remote_copy(
            src_ref=src, dst_ref=dst, send_sem=send, recv_sem=recv,
            device_id=device, device_id_type=MESH,
        )

    def token_copy(k):
        dest = (e, lax.rem(z + k, nz) * CORES + c)
        return (
            remote(meta_ref, metas.at[k], ms.at[k], mr.at[k], dest),
            remote(x_ref, xbuf.at[k], xs.at[k], xr.at[k], dest),
        )

    def row_copy(k, j):
        return remote(
            outbox.at[k, column(j)], rows.at[k, :, c, e], cs.at[k, j], cr.at[k, j], (column(j), t)
        )

    def share_copy(k, j):
        block = rows.at[k, :, c, behind(j)]
        return remote(block, block, ds.at[k, j], dr.at[k, j], partner)

    def share_arrival(k, j):
        block = rows.at[k, :, 1 - c, behind(j)]
        return remote(block, block, ds.at[k, j], dr.at[k, j], partner)

    def pair_copy(k, j):
        return remote(
            rows.at[k, :, 1 - c, column(j)], pair.at[k, j], ps.at[k, j], pr.at[k, j], partner
        )

    def back_copy(k, j):
        return remote(
            rows.at[k, :, c, column(j)], rows_in.at[k, j], bs.at[k, j], br.at[k, j], (column(j), t)
        )

    def final_copy(k):
        dest = (e, lax.rem(z - k + nz, nz) * CORES + c)
        return remote(finalbox.at[k], final.at[k], fs.at[k], fr.at[k], dest)

    order = [0] + sorted(range(1, nz), key=lambda k: -min(k, nz - k))
    columns = [2] + [j for j in range(1, ep) if j != 2] if ep > 2 else list(range(1, ep))
    for k in order[1:]:
        for copy in token_copy(k):
            copy.start()
    loads = [
        pltpu.make_async_copy(source, held, ws.at[n])
        for n, (source, held) in enumerate(
            ((gate_ref, gate_w), (up_ref, up_w), (down_ref, down_w))
        )
    ]
    for load in loads:
        load.start()
    metas[0] = meta_ref[...]

    def select(k):
        if k > 0:
            for copy in token_copy(k):
                copy.wait_recv()
        block = x_ref if k == 0 else xbuf.at[k]
        info = metas[k]
        slot = lax.broadcasted_iota(jnp.int32, (ep * group, tokens), 0).astype(jnp.float32)
        chosen = (slot == info[0:1, :tokens]) | (slot == info[1:2, :tokens])
        picked = jnp.dot(
            jnp.where(chosen, 1.0, 0.0).astype(jnp.bfloat16), block[...],
            preferred_element_type=jnp.float32,
        ).astype(jnp.bfloat16)
        outbox[k] = picked.reshape(ep, local_experts, SLOTS, width)
        for j in columns:
            row_copy(k, j).start()
        rows[k, :, c, e] = outbox[k, e]
        share_copy(k, 0).start()

    def pass_on(k):
        for j in columns:
            row_copy(k, j).wait_recv()
            share_copy(k, j).start()

    def compute(k):
        for j in range(ep):
            share_arrival(k, j).wait_recv()
            share_copy(k, j).wait_send()

        def one_expert(n, carry):
            held = rows[k, n].reshape(CORES * ep * SLOTS, width)
            gate_pre = jnp.minimum(
                jnp.dot(held, gate_w[n], preferred_element_type=jnp.float32), clamp_limit
            )
            up_pre = jnp.clip(
                jnp.dot(held, up_w[n], preferred_element_type=jnp.float32),
                -clamp_limit,
                clamp_limit,
            )
            active = (gate_pre * jax.nn.sigmoid(sig_alpha * gate_pre) * (up_pre + 1.0)).astype(
                jnp.bfloat16
            )
            part = jnp.dot(active, down_w[n], preferred_element_type=jnp.float32)
            rows[k, n] = part.astype(jnp.bfloat16).reshape(CORES, ep, SLOTS, width)
            return carry

        lax.fori_loop(0, local_experts, one_expert, 0)
        for j in columns + [0]:
            pair_copy(k, j).start()

    def add_pairs(k):
        for j in columns + [0]:
            pair_copy(k, j).wait_recv()
            total = (
                rows[k, :, c, column(j)].astype(jnp.float32) + pair[k, j].astype(jnp.float32)
            ).astype(jnp.bfloat16)
            if j > 0:
                rows[k, :, c, column(j)] = total
                back_copy(k, j).start()
            else:
                rows_in[k, 0] = total

    def combine(k):
        for j in columns:
            back_copy(k, j).wait_recv()
        info = metas[k]
        slot = jnp.concatenate(
            [
                (behind(j) * group + lax.broadcasted_iota(jnp.int32, (group, tokens), 0)).astype(
                    jnp.float32
                )
                for j in range(ep)
            ],
            axis=0,
        )
        weight = jnp.where(slot == info[0:1, :tokens], info[2:3, :tokens], 0.0) + jnp.where(
            slot == info[1:2, :tokens], info[3:4, :tokens], 0.0
        )
        high = weight.astype(jnp.bfloat16)
        low = (weight - high.astype(jnp.float32)).astype(jnp.bfloat16)
        held = rows_in[k].reshape(ep * group, width)
        total = jnp.zeros((tokens, width), jnp.float32)
        for piece in (high, low):
            total = total + lax.dot_general(
                piece, held, (((0,), (0,)), ((), ())), preferred_element_type=jnp.float32
            )
        return total

    for k in order:
        select(k)
    for load in loads:
        load.wait()
    for n, k in enumerate(order):
        pass_on(k)
        if n > 0:
            add_pairs(order[n - 1])
        compute(k)
    add_pairs(order[-1])
    total = combine(0)
    for k in order[1:]:
        finalbox[k] = combine(k).astype(jnp.bfloat16)
        final_copy(k).start()
    for k in order[1:]:
        final_copy(k).wait_recv()
        total = total + final[k].astype(jnp.float32)
    out_ref[...] = total.astype(jnp.bfloat16)
    for k in range(nz):
        if k > 0:
            final_copy(k).wait_send()
            for copy in token_copy(k):
                copy.wait_send()
        for j in range(ep):
            pair_copy(k, j).wait_send()
            if j > 0:
                row_copy(k, j).wait_send()
                back_copy(k, j).wait_send()


def run_experts(x, meta, gate_weight, up_weight, down_weight, ep, nz):
    local_experts = gate_weight.shape[0]
    width = x.shape[1]
    dma = pltpu.SemaphoreType.DMA
    box = (nz, ep, local_experts, SLOTS, width)
    vmem = pl.BlockSpec(memory_space=pltpu.VMEM)
    held = pl.BlockSpec(memory_space=pl.ANY)
    return pl.pallas_call(
        functools.partial(expert_kernel, ep, nz, local_experts),
        out_shape=jax.ShapeDtypeStruct(x.shape, jnp.bfloat16),
        in_specs=[vmem, vmem, held, held, held],
        out_specs=vmem,
        scratch_shapes=[
            pltpu.VMEM((nz,) + meta.shape, jnp.float32),
            pltpu.VMEM((nz,) + x.shape, jnp.bfloat16),
            pltpu.VMEM(box, jnp.bfloat16),
            pltpu.VMEM((nz, local_experts, CORES, ep, SLOTS, width), jnp.bfloat16),
            pltpu.VMEM(box, jnp.bfloat16),
            pltpu.VMEM(box, jnp.bfloat16),
            pltpu.VMEM((nz,) + x.shape, jnp.bfloat16),
            pltpu.VMEM((nz,) + x.shape, jnp.bfloat16),
            pltpu.VMEM(gate_weight.shape, jnp.bfloat16),
            pltpu.VMEM(up_weight.shape, jnp.bfloat16),
            pltpu.VMEM(down_weight.shape, jnp.bfloat16),
            dma((nz,)), dma((nz,)), dma((nz,)), dma((nz,)),
            dma((nz, ep)), dma((nz, ep)), dma((nz, ep)), dma((nz, ep)),
            dma((nz, ep)), dma((nz, ep)), dma((nz, ep)), dma((nz, ep)),
            dma((nz,)), dma((nz,)), dma((3,)),
        ],
        compiler_params=pltpu.CompilerParams(
            collective_id=0, has_side_effects=True, vmem_limit_bytes=63 * 1024 * 1024
        ),
        cost_estimate=pl.CostEstimate(
            flops=60_000_000_000, bytes_accessed=20_000_000, transcendentals=0
        ),
    )(x, meta, gate_weight, up_weight, down_weight)


def local(
    queries, key_vectors, value_vectors, cumulative_gate, out_weight, expert_tokens, norm_gain,
    gate_weight, up_weight, down_weight, expert_choice, route_weights,
):
    ep, nz = lax.axis_size("ep"), lax.axis_size("tp") // CORES
    tokens, width = expert_tokens.shape
    local_experts = gate_weight.shape[0]
    gate_high = lax.reduce_precision(cumulative_gate, 8, 7)
    gate_rest = cumulative_gate - gate_high
    gate_mid = lax.reduce_precision(gate_rest, 8, 7)
    gate_low = gate_rest - gate_mid
    keyed = jnp.concatenate(
        [key_vectors]
        + [piece.astype(jnp.bfloat16) for piece in (gate_high, gate_mid, gate_low)],
        axis=1,
    )
    all_keyed = lax.all_gather(keyed, "ep", axis=0, tiled=True)
    value_rows = lax.all_gather(value_vectors, "ep", axis=0, tiled=True)

    tokens_float = expert_tokens.astype(jnp.float32)
    normed = (
        tokens_float
        * lax.rsqrt(jnp.mean(tokens_float * tokens_float, axis=1, keepdims=True) + eps_norm)
        * norm_gain
    ).astype(jnp.bfloat16)
    flat_ids = expert_choice.reshape(-1)
    one_hot = (flat_ids[:, None] == jnp.arange(ep * local_experts, dtype=jnp.int32)[None, :]).astype(
        jnp.float32
    )
    position = jnp.arange(flat_ids.shape[0], dtype=jnp.int32)
    earlier = (position[:, None] > position[None, :]).astype(jnp.float32)
    slot_rank = jnp.sum(jnp.dot(earlier, one_hot) * one_hot, axis=1)
    slot_ids = (flat_ids.astype(jnp.float32) * SLOTS + slot_rank).reshape(tokens, -1)
    meta = jnp.concatenate([slot_ids.T, route_weights.T], axis=0)
    meta = jnp.pad(meta, ((0, 8 - meta.shape[0]), (0, -tokens % 128)), constant_values=-1.0)

    kept = queries.shape[1]
    heads_here = cumulative_gate.shape[1]
    key_rows = all_keyed[:, :kept]
    pieces = all_keyed[:, kept:].astype(jnp.float32)
    gate_rows = (
        pieces[:, :heads_here] + pieces[:, heads_here : 2 * heads_here]
    ) + pieces[:, 2 * heads_here :]
    block_rows = queries.shape[0]
    first_query = lax.axis_index("ep") * block_rows
    query_pos = first_query + jnp.arange(block_rows, dtype=jnp.int32)
    last_query = first_query + block_rows - 1
    carried = (
        jnp.full((heads_here, block_rows), floor_score, jnp.float32),
        jnp.zeros((heads_here, block_rows), jnp.float32),
        jnp.zeros((block_rows, kept), jnp.float32),
    )

    def one_shard(inner_state, shard_index):
        offset = shard_index * block_rows
        shard_keys = lax.dynamic_slice_in_dim(key_rows, offset, block_rows, 0)
        shard_values = lax.dynamic_slice_in_dim(value_rows, offset, block_rows, 0)
        shard_gates = lax.dynamic_slice_in_dim(gate_rows, offset, block_rows, 0)
        updated = lax.cond(
            offset <= last_query,
            lambda held_state: attend_shard(
                held_state, queries, cumulative_gate, query_pos, shard_keys, shard_values,
                shard_gates, offset,
            ),
            lambda held_state: held_state,
            inner_state,
        )
        return (updated, None)

    carried, unused = lax.scan(one_shard, carried, jnp.arange(ep, dtype=jnp.int32))
    final_peak, final_sum, final_accum = carried
    attention = (
        (final_accum.reshape(block_rows, heads_here, -1) / final_sum.T[:, :, None])
        .reshape(block_rows, -1)
        .astype(jnp.bfloat16)
    )
    mixed = head_term(attention, out_weight).astype(jnp.bfloat16)
    normed, meta, mixed = lax.optimization_barrier((normed, meta, mixed))
    mixer_output = lax.psum_scatter(mixed, "tp", scatter_dimension=0, tiled=True)
    expert_output = run_experts(normed, meta, gate_weight, up_weight, down_weight, ep, nz)
    return (mixer_output, expert_output)


def solution(mesh):
    placed = (
        P("ep", "tp"),
        P("ep", "tp"),
        P("ep", "tp"),
        P("ep", "tp"),
        P("tp", None),
        P(("ep", "tp"), None),
        P(),
        P("ep", None, "tp"),
        P("ep", None, "tp"),
        P("ep", "tp", None),
        P(("ep", "tp"), None),
        P(("ep", "tp"), None),
    )
    return jax.shard_map(
        local,
        mesh=mesh,
        in_specs=placed,
        out_specs=(P(("ep", "tp"), None), P(("ep", "tp"), None)),
        check_vma=False,
    )
```

time: 195 us -> 213 us (1.092)
  the two profiles are of different devices: /device:TPU:0 before, /device:TPU:28 now
where the time goes in v2:
time: 213 us
  Pallas kernels  140 us (66%)
  blocking collectives  21.5 us (10%)
  matrix products  18.7 us (9%)
  between operations  14.2 us (7%)
  local copies, waits for them, and re-layouts  7.92 us (4%)
  other arithmetic  7.03 us (3%)
  loops' own time  2.95 us (1%)
    pallas_call x1, Pallas kernels, run_experts(): pl.pallas_call(functools.partial(expert_kernel, ep, nz, local_experts), o...  140 us
    all_gather x1, blocking collectives, local(): value_rows = lax.all_gather(value_vectors, 'ep', axis=0, tiled=True)  11.4 us
    all_gather x1, blocking collectives, local(): all_keyed = lax.all_gather(keyed, 'ep', axis=0, tiled=True)  10.1 us
    dot_general x6, matrix products, attend_shard(): jnp.einsum('qd,kd->qk', queries[:, first_column:last_column], key_rows[:,...  8.39 us
    dot_general x6, matrix products, attend_shard(): jnp.dot(weights.astype(jnp.bfloat16), value_rows[:, first_column:last_col...  8.12 us
  transfers between devices with their start and end apart: 1, of which 0 were waited for; matrix products, arithmetic and copies ran while one was open for 0% of the time, Pallas kernels for 66%

profile of v2, /device:TPU:28, one launch (start us, length us, event | category | flops | bytes accessed | tf_op | source)
XLA Modules:
  0.0 212.7 jit_solution(13153650718095103534)
XLA Ops:
  7.2 0.0 copy-start
  7.2 0.0 copy-start.2
  7.2 0.0 reduce-scatter.2.cloned.1.call-start
  7.2 0.7 reduce-precision_convert_fusion.1
  8.0 1.0 copy.18
  9.0 10.1 %all_gather.6 = bf16[2048,134]{0,1:T(8,128)(2,1)S(1)} all-gather(bf16[512,134]{0,1:T(8,128)(2,1)S(1)} %pad_maximum_fusion.3), channel_id=1, replica_groups=mesh['ep'=4,'tp'=8] {'ep'}, dimensions={0}, use_global_device_ids=true | all-gather | bytes 686080 | tf_op jit(solution)/shard_map/all_gather | solution.py:325
  19.2 1.0 copy.19
  20.3 11.4 %all_gather.7 = bf16[2048,128]{1,0:T(8,128)(2,1)} all-gather(bf16[512,128]{1,0:T(8,128)(2,1)} %param.18), channel_id=1, replica_groups=mesh['ep'=4,'tp'=8] {'ep'}, dimensions={0}, use_global_device_ids=true | all-gather | bytes 655360 | tf_op jit(solution)/shard_map/all_gather | solution.py:326
  31.6 0.7 broadcast_in_dim.38
  32.4 0.0 copy-done.2
  32.4 0.0 copy-start.1
  32.4 0.0 copy-start.4
  32.4 0.0 copy-start.3
  32.4 25.9 %while.15 = (s32[]{:T(128)}, f32[2,512]{1,0:T(2,128)S(1)}, f32[2,512]{1,0:T(2,128)S(1)}, f32[512,128]{0,1:T(8,128)}, s32[4]{0:T(128)S(1)}, /*index=5*/s32[]{:T(1...) while((s32[]{:T(128)}, f32[2,512]{1,0:T(2,128)S(1)}, ...), condition=%wide.region_9.10_spmd.clone, body=%wide.region_2.9_spmd.clone.sunk | while | flops 141499392 | bytes 8266141 | solution.py:378
  32.4 0.6 dynamic_slice.33
  33.7 6.9 %conditional.3 = ((f32[2,512]{1,0:T(2,128)S(1)}, f32[2,512]{1,0:T(2,128)S(1)}, f32[512,128]{0,1:T(8,128)})) conditional(s32[]{:T(128)} %convert_element_type.76, (f32[2,512]{1,0:T(2,128)S(1)}, f32[2,512]{1,0:T(2,128)S(1)}, f32[512,128]{0,1:T(8,128)}) %tuple.66, (f32[2,512]{1,0:T(2,128)S(1)}, s32[]{:T(128)}, s32[]{:T(128)}, ...), branch_computations={%region_3.3_spmd, %region_4.8_spmd} | conditional | flops 141499392 | bytes 8263810 | solution.py:367
  33.8 0.1 fusion.39
  33.8 1.4 fusion.42
  35.2 1.3 convolution_add_fusion.1
  36.6 1.4 fusion.43
  38.0 1.4 convolution_add_fusion
  39.4 0.7 pad_maximum_fusion
  40.1 0.4 fusion.9
  40.6 0.6 dynamic_slice.33
  41.9 6.9 %conditional.3 = ((f32[2,512]{1,0:T(2,128)S(1)}, f32[2,512]{1,0:T(2,128)S(1)}, f32[512,128]{0,1:T(8,128)})) conditional(s32[]{:T(128)} %convert_element_type.76, (f32[2,512]{1,0:T(2,128)S(1)}, f32[2,512]{1,0:T(2,128)S(1)}, f32[512,128]{0,1:T(8,128)}) %tuple.66, (f32[2,512]{1,0:T(2,128)S(1)}, s32[]{:T(128)}, s32[]{:T(128)}, ...), branch_computations={%region_3.3_spmd, %region_4.8_spmd} | conditional | flops 141499392 | bytes 8263810 | solution.py:367
  41.9 0.1 fusion.39
  42.0 1.4 fusion.42
  43.4 1.3 convolution_add_fusion.1
  44.7 1.4 fusion.43
  46.2 1.4 convolution_add_fusion
  47.6 0.7 pad_maximum_fusion
  48.3 0.4 fusion.9
  48.8 0.6 dynamic_slice.33
  50.1 6.9 %conditional.3 = ((f32[2,512]{1,0:T(2,128)S(1)}, f32[2,512]{1,0:T(2,128)S(1)}, f32[512,128]{0,1:T(8,128)})) conditional(s32[]{:T(128)} %convert_element_type.76, (f32[2,512]{1,0:T(2,128)S(1)}, f32[2,512]{1,0:T(2,128)S(1)}, f32[512,128]{0,1:T(8,128)}) %tuple.66, (f32[2,512]{1,0:T(2,128)S(1)}, s32[]{:T(128)}, s32[]{:T(128)}, ...), branch_computations={%region_3.3_spmd, %region_4.8_spmd} | conditional | flops 141499392 | bytes 8263810 | solution.py:367
  50.1 0.1 fusion.39
  50.2 1.4 fusion.42
  51.6 1.3 convolution_add_fusion.1
  52.9 1.4 fusion.43
  54.4 1.4 convolution_add_fusion
  55.8 0.7 pad_maximum_fusion
  56.5 0.4 fusion.9
  57.0 0.6 dynamic_slice.33
  58.3 0.0 copy-done.1
  58.3 0.0 copy-start.5
  58.3 0.2 fusion.33
  58.5 0.0 copy-done.4
  58.5 0.1 copy.16
  58.6 0.1 eq.15
  58.8 0.2 fusion.32
  58.9 0.2 reduce_sum.50
  59.1 0.1 copy.17
  59.2 1.0 fusion.36
  60.2 0.0 copy-done
  60.2 2.1 convolution_convert_fusion
  62.3 0.0 copy-done.3
  62.3 0.9 fusion.35.x_ref
  63.2 0.0 copy-done.5
  63.2 0.6 select_maximum_fusion.meta_ref
  63.8 0.0 reduce-scatter.2.cloned.1.call-update
  63.8 140.2 %shard_map.131 = bf16[96,2048]{1,0:T(8,128)(2,1)} custom-call(bf16[96,2048]{1,0:T(8,128)(2,1)} %fusion.35.x_ref, f32[8,128]{1,0:T(8,128)} %select_maximum_fusion.meta_ref, bf16[4,2048,256]{2,1,0:T(8,128)(2,1)} %gate_ref.1, bf16[4,2048,256]{2,1,0:T(8,128)(2,1)} %up_ref.1, bf16[4,256,2048]{2,1,0:T(8,128)(2,1)} %down_ref.1), custom_call_target="tpu_custom_call" | custom-call | flops 60000002048 | bytes 20000000 | tf_op jit(solution)/shard_map/pallas_call | solution.py:278
  204.0 0.0 reduce-scatter.2.cloned.1.call-done
  204.0 1.8 copy.41
  (35 shorter events, 0.3 us)
Async XLA Ops:
  7.2 53.0 %copy-start = (bf16[128,2048]{1,0:T(8,128)(2,1)S(1)}, bf16[128,2048]{1,0:T(8,128)(2,1)}, u32[]{:S(2)}) copy-start(bf16[128,2048]{1,0:T(8,128)(2,1)} %param.20) | copy-start | bytes 1572868
  7.2 25.2 %copy-start.2 = (f32[512,2]{0,1:T(2,128)S(1)}, f32[512,2]{0,1:T(2,128)}, u32[]{:S(2)}) copy-start(f32[512,2]{0,1:T(2,128)} %param.19) | copy-start | bytes 12292
  7.2 196.8 %reduce-scatter.2.cloned.1.call-start = ((), (), s32[]{:S(2)}) async-start(), calls=%async_computation.1 | async-start | bytes 2359296 | tf_op jit(solution)/shard_map/reduce_scatter | solution.py:387
  32.4 25.9 %copy-start.1 = (bf16[96,2048]{1,0:T(8,128)(2,1)S(1)}, bf16[96,2048]{1,0:T(8,128)(2,1)}, u32[]{:S(2)}) copy-start(bf16[96,2048]{1,0:T(8,128)(2,1)} %param.21) | copy-start | bytes 1179652
  32.4 26.1 %copy-start.4 = (s32[96,2]{0,1:T(2,128)S(1)}, s32[96,2]{0,1:T(2,128)}, u32[]{:S(2)}) copy-start(s32[96,2]{0,1:T(2,128)} %param.26) | copy-start | bytes 2308
  32.4 29.9 %copy-start.3 = (f32[2048]{0:T(1024)S(1)}, f32[2048]{0:T(1024)}, u32[]{:S(2)}) copy-start(f32[2048]{0:T(1024)} %param.22) | copy-start | bytes 24580
  58.3 4.8 %copy-start.5 = (f32[96,2]{0,1:T(2,128)S(1)}, f32[96,2]{0,1:T(2,128)}, u32[]{:S(2)}) copy-start(f32[96,2]{0,1:T(2,128)} %param.27) | copy-start | bytes 2308
Sparse Core Ops, SparseCore 0:
  63.9 60.7 reduce-scatter.1
